TPU v7x, 32 devices: a whole 2x2x4 slice. The times are simulated.
32 devices in a mesh: grp: 2 (over y), fs: 4 (over z), tp: 4 (over x, core).
Axes of the slice: x: 2, y: 2, z: 4, core: 2. Of those that a mesh axis runs over, the one named last changes fastest.
Arguments:
- tokens: bfloat16 [8, 384, 2048], P(('grp', 'fs'), None, 'tp'), parts along dimension 0, may hold values from -16 to 16
- norm_gain: float32 [2048], P('tp'), may hold values from 0.1 to 1.9
- in_weight: bfloat16 [2048, 1024], P('fs', 'tp'), may hold values from -0.125 to 0.125
- pool_weight: bfloat16 [8, 128, 128], P('tp'), may hold values from -0.5 to 0.5
- pool_scale: float32 [1024], P('tp'), may hold values from 0.1 to 1.9
- out_weight: bfloat16 [1024, 2048], P('fs', 'tp'), may hold values from -0.1875 to 0.1875
- ffn_gain: float32 [2048], P('tp'), may hold values from 0.1 to 1.9
- gate_weight: bfloat16 [2048, 5632], P('fs', 'tp'), may hold values from -0.125 to 0.125
- up_weight: bfloat16 [2048, 5632], P('fs', 'tp'), may hold values from -0.125 to 0.125
- down_weight: bfloat16 [5632, 2048], P('tp', 'fs'), may hold values from -0.078125 to 0.078125
Outputs:
- output: bfloat16 [8, 384, 2048], P(('grp', 'fs'), None, 'tp'), parts along dimension 0
There are 2 independent parts, one for each index of `grp`. A program takes and returns all parts, laid end to end along the dimension named above; an argument that names none is the same for every part. Nothing has to cross between parts.
All inputs are finite; a program needn't handle non-finite values.
Results may differ from a plain program's by a relative error of at most 0.009.
Values may be sent and summed in bfloat16 or wider, within the bound.
A program may use at most 64 MiB of HBM per device.

v0:
```python
import jax
import jax.numpy as jnp
from jax import lax
from jax.sharding import PartitionSpec as P

D = 2048
GD = 128
EPSILON = 0.05
HALVES = (1, 2, 4, 8)


def local(
    tokens,
    norm_gain,
    in_weight,
    pool_weight,
    pool_scale,
    out_weight,
    ffn_gain,
    gate_weight,
    up_weight,
    down_weight,
):
    seq_local, length, feat_local = tokens.shape
    stream = tokens.astype(jnp.float32)
    first_square = lax.psum(jnp.sum(stream * stream, axis=-1), "tp")
    normed = (stream * lax.rsqrt(first_square[..., None] / D + EPSILON) * norm_gain).astype(
        jnp.bfloat16
    )
    in_full = lax.all_gather(in_weight, "fs", axis=0, tiled=True)
    channels = in_full.shape[1]
    weight_rows = in_full
    pool_input = jnp.einsum(
        "slk,kc->slc",
        lax.all_gather(normed, "tp", axis=2, tiled=True),
        weight_rows,
        preferred_element_type=jnp.float32,
    ).astype(jnp.bfloat16)
    pool_float = pool_input.astype(jnp.float32)
    group_local = pool_weight.shape[0]
    group_ids = lax.axis_index("tp") * group_local + jnp.arange(channels) // GD
    selector = group_ids % 4
    running = jnp.concatenate(
        [jnp.zeros((seq_local, 1, channels), jnp.float32), jnp.cumsum(pool_float, axis=1)], axis=1
    )
    position = jnp.arange(length)
    window_mean = jnp.zeros_like(pool_float)
    for window_index, half_width in enumerate(HALVES):
        upper_sum = jnp.concatenate(
            [running[:, half_width:], jnp.repeat(running[:, -1:], half_width, axis=1)], axis=1
        )[:, :length]
        lower_sum = jnp.concatenate(
            [
                jnp.zeros((seq_local, half_width, channels), jnp.float32),
                running[:, : length + 1 - half_width],
            ],
            axis=1,
        )[:, :length]
        counts = (
            jnp.minimum(position + half_width, length) - jnp.maximum(position - half_width, 0)
        ).astype(jnp.float32)
        window_mean = jnp.where(
            selector == window_index, (upper_sum - lower_sum) / counts[:, None], window_mean
        )
    deviation = (window_mean - pool_float).astype(jnp.bfloat16)
    grouped = deviation.reshape(seq_local, length, group_local, GD)
    mapped = jnp.einsum("slgc,gcd->slgd", grouped, pool_weight, preferred_element_type=jnp.float32)
    pooled = (mapped.reshape(seq_local, length, channels) * pool_scale).astype(jnp.bfloat16)
    out_full = lax.all_gather(out_weight, "fs", axis=0, tiled=True)
    weight_rows = out_full
    mixed = stream + jnp.einsum(
        "jut,tx->jux",
        lax.all_gather(pooled, "tp", axis=2, tiled=True),
        weight_rows,
        preferred_element_type=jnp.float32,
    )
    second_square = lax.psum(jnp.sum(mixed * mixed, axis=-1), "tp")
    normed_two = (mixed * lax.rsqrt(second_square[..., None] / D + EPSILON) * ffn_gain).astype(
        jnp.bfloat16
    )
    features_full = lax.all_gather(normed_two, "tp", axis=2, tiled=True)
    gate_sum = jnp.einsum(
        "slk,kf->slf",
        features_full,
        lax.all_gather(gate_weight, "fs", axis=0, tiled=True),
        preferred_element_type=jnp.float32,
    )
    up_sum = jnp.einsum(
        "slk,kf->slf",
        features_full,
        lax.all_gather(up_weight, "fs", axis=0, tiled=True),
        preferred_element_type=jnp.float32,
    )
    hidden = (jax.nn.silu(gate_sum) * up_sum).astype(jnp.bfloat16)
    partial_value = jnp.einsum(
        "hor,rn->hon",
        hidden,
        lax.all_gather(down_weight, "fs", axis=1, tiled=True),
        preferred_element_type=jnp.float32,
    )
    summed = lax.psum_scatter(
        partial_value.astype(jnp.bfloat16), "tp", scatter_dimension=2, tiled=True
    ).astype(jnp.float32)
    return (mixed + summed).astype(jnp.bfloat16)


def solution(mesh):
    return jax.shard_map(
        local,
        mesh=mesh,
        in_specs=(
            P(("grp", "fs"), None, "tp"),
            P("tp"),
            P("fs", "tp"),
            P("tp", None, None),
            P("tp"),
            P("fs", "tp"),
            P("tp"),
            P("fs", "tp"),
            P("fs", "tp"),
            P("tp", "fs"),
        ),
        out_specs=P(("grp", "fs"), None, "tp"),
        check_vma=False,
    )
```

profile of v0, /device:TPU:0, one launch (start us, length us, event | category | flops | bytes accessed | tf_op | source)
XLA Modules:
  0.0 485.2 jit_solution(12671679941246397171)
XLA Ops:
  6.5 0.0 copy-start
  6.5 0.0 all-gather.10.cloned.1.call-start
  6.5 0.7 all-gather.10.cloned.1.call-update
  7.3 0.0 all-gather.8.cloned.1.call-start
  7.3 1.2 fusion.17
  8.5 8.4 %psum.14 = f32[1,384]{1,0:T(1,128)S(1)} all-reduce(f32[1,384]{1,0:T(1,128)S(1)} %reduce_sum.23), channel_id=1, replica_groups=mesh['grp'=2,'fs'=4,'tp'=4] {'tp'}, use_global_device_ids=true, to_apply=%region_1.0 | all-reduce | flops 384 | bytes 3072 | tf_op jit(solution)/shard_map/psum | solution.py:26
  16.9 1.9 fusion.19
  18.8 0.0 all-gather.8.cloned.1.call-update
  18.8 0.0 all-gather.12.cloned.1.call-start
  18.8 0.7 all-gather.12.cloned.1.call-update
  19.5 0.0 all-gather.14.cloned.1.call-start
  19.6 20.0 %all-gather.10.cloned.1.call-done = bf16[2048,256]{1,0:T(8,128)(2,1)} async-done(((bf16[512,256]{1,0:T(8,128)(2,1)}), bf16[2048,256]{1,0:T(8,128)(2,1)}) %all-gather.10.cloned.1.call-update) | async-done | bytes 1048592 | tf_op jit(solution)/shard_map/all_gather | solution.py:30
  39.6 20.6 %all-gather.8.cloned.1.call-done = bf16[1,384,2048]{2,1,0:T(8,128)(2,1)} async-done(((bf16[1,384,512]{2,1,0:T(8,128)(2,1)}), bf16[1,384,2048]{2,1,0:T(8,128)(2,1)}) %all-gather.8.cloned.1.call-update) | async-done | bytes 1572880 | tf_op jit(solution)/shard_map/all_gather | solution.py:35
  60.2 2.3 fusion.14
  62.5 0.3 fusion.23
  62.8 0.1 copy.12
  63.0 0.1 fusion.63
  63.1 0.1 fusion.61
  63.1 0.1 fusion.62
  63.2 0.0 copy-start.3
  63.3 0.5 fusion.39
  63.8 0.0 copy-start.1
  63.8 0.1 reshape.225
  63.8 0.0 copy-done
  63.8 0.3 fusion.40
  64.1 0.0 copy-done.3
  64.1 0.1 fusion.38
  64.2 0.0 copy-start.2
  64.2 8.6 %all_gather.26 = bf16[1,384,1024]{1,2,0:T(8,128)(2,1)S(1)} all-gather(bf16[1,384,256]{1,2,0:T(8,128)(2,1)S(1)} %fusion.38), channel_id=1, replica_groups=mesh['grp'=2,'fs'=4,'tp'=4] {'tp'}, dimensions={2}, use_global_device_ids=true | all-gather | bytes 983040 | tf_op jit(solution)/shard_map/all_gather | solution.py:73
  72.8 17.0 %all-gather.12.cloned.1.call-done = bf16[1024,512]{1,0:T(8,128)(2,1)} async-done(((bf16[256,512]{1,0:T(8,128)(2,1)}), bf16[1024,512]{1,0:T(8,128)(2,1)}) %all-gather.12.cloned.1.call-update) | async-done | bytes 1048592 | tf_op jit(solution)/shard_map/all_gather | solution.py:69
  89.8 0.0 copy-done.1
  89.8 1.9 multiply_reduce_fusion
  91.8 6.1 %psum.15 = f32[1,384]{1,0:T(1,128)S(1)} all-reduce(f32[1,384]{1,0:T(1,128)S(1)} %reduce_sum.25), channel_id=1, replica_groups=mesh['grp'=2,'fs'=4,'tp'=4] {'tp'}, use_global_device_ids=true, to_apply=%region_5.6 | all-reduce | flops 384 | bytes 3072 | tf_op jit(solution)/shard_map/psum | solution.py:77
  97.9 0.0 copy-done.2
  97.9 0.9 multiply_convert_fusion
  98.8 0.0 all-gather.14.cloned.1.call-update
  98.8 0.0 all-gather.16.cloned.1.call-start
  98.8 0.5 all-gather.16.cloned.1.call-update
  99.4 0.0 all-gather.18.cloned.1.call-start
  99.4 0.5 all-gather.18.cloned.1.call-update
  99.9 0.0 all-gather.20.cloned.1.call-start
  100.0 0.7 all-gather.20.cloned.1.call-update
  100.7 0.0 reduce-scatter.2.cloned.1.call-start
  100.7 17.0 %all-gather.14.cloned.1.call-done = bf16[1,384,2048]{2,1,0:T(8,128)(2,1)} async-done(((bf16[1,384,512]{2,1,0:T(8,128)(2,1)}), bf16[1,384,2048]{2,1,0:T(8,128)(2,1)}) %all-gather.14.cloned.1.call-update) | async-done | bytes 1572880 | tf_op jit(solution)/shard_map/all_gather | solution.py:81
  117.8 0.0 copy-start.4
  117.8 108.1 %all-gather.16.cloned.1.call-done = bf16[2048,1408]{1,0:T(8,128)(2,1)} async-done(((bf16[512,1408]{1,0:T(8,128)(2,1)}), bf16[2048,1408]{1,0:T(8,128)(2,1)}) %all-gather.16.cloned.1.call-update) | async-done | bytes 5767184 | tf_op jit(solution)/shard_map/all_gather | solution.py:85
  225.9 7.1 %fusion.3 = f32[384,1408]{1,0:T(8,128)} fusion(bf16[2048,1408]{1,0:T(8,128)(2,1)} %all-gather.16.cloned.1.call-done, bf16[1,384,2048]{2,1,0:T(8,128)(2,1)} %all-gather.14.cloned.1.call-done), kind=kOutput, calls=%fused_computation.5 | convolution fusion | flops 2214592512 | bytes 9502720 | tf_op jit(solution)/shard_map/slk,kf->slf/dot_general | solution.py:82
  233.0 99.3 %all-gather.18.cloned.1.call-done = bf16[2048,1408]{1,0:T(8,128)(2,1)} async-done(((bf16[512,1408]{1,0:T(8,128)(2,1)}), bf16[2048,1408]{1,0:T(8,128)(2,1)}) %all-gather.18.cloned.1.call-update) | async-done | bytes 5767184 | tf_op jit(solution)/shard_map/all_gather | solution.py:91
  332.3 106.5 %all-gather.20.cloned.1.call-done = bf16[1408,2048]{1,0:T(8,128)(2,1)} async-done(((bf16[1408,512]{1,0:T(8,128)(2,1)}), bf16[1408,2048]{1,0:T(8,128)(2,1)}) %all-gather.20.cloned.1.call-update) | async-done | bytes 5767184 | tf_op jit(solution)/shard_map/all_gather | solution.py:98
  438.9 0.0 copy-done.4
  438.9 11.3 %fusion.1 = bf16[1,384,2048]{2,1,0:T(8,128)(2,1)} fusion(bf16[1408,2048]{1,0:T(8,128)(2,1)} %all-gather.20.cloned.1.call-done, bf16[2048,1408]{1,0:T(8,128)(2,1)} %all-gather.18.cloned.1.call-done, f32[384,1408]{1,0:T(8,128)} %fusion.3, bf16[1,384,2048]{2,1,0:T(8,128)(2,1)S(1)} %copy-done.4), kind=kOutput, calls=%fused_computation.3 | convolution fusion | flops 4433215488 | bytes 16842752 | tf_op jit(solution)/shard_map/hor,rn->hon/dot_general | solution.py:95
  450.1 0.0 reduce-scatter.2.cloned.1.call-update
  450.2 26.4 %reduce-scatter.2.cloned.1.call-done = bf16[1,384,512]{2,1,0:T(8,128)(2,1)} async-done(((bf16[1,384,2048]{2,1,0:T(8,128)(2,1)}), bf16[1,384,512]{2,1,0:T(8,128)(2,1)}) %reduce-scatter.2.cloned.1.call-update) | async-done | bytes 393232 | tf_op jit(solution)/shard_map/reduce_scatter | solution.py:101
  476.5 1.9 add_convert_fusion
  (17 shorter events, 0.2 us)
Async XLA Ops:
  6.5 57.3 %copy-start = (bf16[2,128,128]{2,1,0:T(8,128)(2,1)S(1)}, bf16[2,128,128]{2,1,0:T(8,128)(2,1)}, u32[]{:S(2)}) copy-start(bf16[2,128,128]{2,1,0:T(8,128)(2,1)} %param.13) | copy-start | bytes 196612
  6.5 33.1 %all-gather.10.cloned.1.call-start = ((), (), s32[]{:S(2)}) async-start(), calls=%async_computation.2 | async-start | bytes 1310720 | tf_op jit(solution)/shard_map/all_gather | solution.py:30
  7.3 53.0 %all-gather.8.cloned.1.call-start = ((), (), s32[]{:S(2)}) async-start(), calls=%async_computation.1 | async-start | bytes 1966080 | tf_op jit(solution)/shard_map/all_gather | solution.py:35
  18.8 71.0 %all-gather.12.cloned.1.call-start = ((), (), s32[]{:S(2)}) async-start(), calls=%async_computation.3 | async-start | bytes 1310720 | tf_op jit(solution)/shard_map/all_gather | solution.py:69
  19.5 98.3 %all-gather.14.cloned.1.call-start = ((), (), s32[]{:S(2)}) async-start(), calls=%async_computation.4 | async-start | bytes 1966080 | tf_op jit(solution)/shard_map/all_gather | solution.py:81
  63.2 0.9 copy-start.3
  63.8 26.1 %copy-start.1 = (bf16[1,384,512]{2,1,0:T(8,128)(2,1)S(1)}, bf16[1,384,512]{2,1,0:T(8,128)(2,1)}, u32[]{:S(2)}) copy-start(bf16[1,384,512]{2,1,0:T(8,128)(2,1)} %param.10) | copy-start | bytes 1179652
  64.2 33.6 %copy-start.2 = (f32[512]{0:T(512)S(1)}, f32[512]{0:T(512)}, u32[]{:S(2)}) copy-start(f32[512]{0:T(512)} %param.16) | copy-start | bytes 6148
  98.8 127.2 %all-gather.16.cloned.1.call-start = ((), (), s32[]{:S(2)}) async-start(), calls=%async_computation.5 | async-start | bytes 7208960 | tf_op jit(solution)/shard_map/all_gather | solution.py:85
  99.4 233.0 %all-gather.18.cloned.1.call-start = ((), (), s32[]{:S(2)}) async-start(), calls=%async_computation.6 | async-start | bytes 7208960 | tf_op jit(solution)/shard_map/all_gather | solution.py:91
  99.9 338.9 %all-gather.20.cloned.1.call-start = ((), (), s32[]{:S(2)}) async-start(), calls=%async_computation.7 | async-start | bytes 7208960 | tf_op jit(solution)/shard_map/all_gather | solution.py:98
  100.7 375.8 %reduce-scatter.2.cloned.1.call-start = ((), (), s32[]{:S(2)}) async-start(), calls=%async_computation.8 | async-start | bytes 1966080 | tf_op jit(solution)/shard_map/reduce_scatter | solution.py:101
  117.8 321.1 %copy-start.4 = (bf16[1,384,2048]{2,1,0:T(8,128)(2,1)S(1)}, bf16[1,384,2048]{2,1,0:T(8,128)(2,1)}, u32[]{:S(2)}) copy-start(bf16[1,384,2048]{2,1,0:T(8,128)(2,1)} %all-gather.14.cloned.1.call-done) | copy-start | bytes 4718596
Sparse Core Ops, SparseCore 0:
  8.9 30.6 all-gather.9
  41.2 18.9 all-gather.7
  61.8 27.9 all-gather.11
  98.9 18.8 all-gather.13
  119.2 106.6 all-gather.15
  227.4 104.9 all-gather.17
  333.9 104.9 all-gather.19
  450.3 26.2 reduce-scatter.1
where the time goes:
time: 486 us; the launch traced here: 485 us
  waiting for transfers between devices  418 us (86%)
  blocking collectives  23 us (5%)
  matrix products  22.8 us (5%)
  between operations  13.7 us (3%)
  other arithmetic  6.86 us (1%)
    all_gather x1, waiting for transfers between devices, local(): lax.all_gather(gate_weight, 'fs', axis=0, tiled=True)  108 us
    all_gather x1, waiting for transfers between devices, local(): lax.all_gather(down_weight, 'fs', axis=1, tiled=True)  107 us
    all_gather x1, waiting for transfers between devices, local(): lax.all_gather(up_weight, 'fs', axis=0, tiled=True)  99.3 us
    reduce_scatter x1, waiting for transfers between devices, local(): lax.psum_scatter(partial_value.astype(jnp.bfloat16), 'tp', scatter_dimens...  26.4 us
    all_gather x1, waiting for transfers between devices, local(): lax.all_gather(normed, 'tp', axis=2, tiled=True)  20.6 us
    all_gather x1, waiting for transfers between devices, local(): in_full = lax.all_gather(in_weight, 'fs', axis=0, tiled=True)  20 us
    all_gather x1, waiting for transfers between devices, local(): features_full = lax.all_gather(normed_two, 'tp', axis=2, tiled=True)  17 us
    all_gather x1, waiting for transfers between devices, local(): out_full = lax.all_gather(out_weight, 'fs', axis=0, tiled=True)  17 us
  transfers between devices with their start and end apart: 8, of which 8 were waited for; matrix products, arithmetic and copies ran while one was open for 3% of the time, Pallas kernels for 0%

commit v1 on v0

--- a/solution.py
+++ b/solution.py
@@ -21,6 +21,23 @@
     up_weight,
     down_weight,
 ):
+
+    def _trace_node(sample, net_axis, arr):
+        r1 = lax.axis_size(net_axis)
+        local_part = lax.axis_index(net_axis)
+        val, all_rows, seen_now = (r1, local_part, sample.shape[1])
+        chunks = []
+        for p in [*range(val)]:
+            t_next = (
+                lax.ppermute(sample, net_axis, [(rr, (rr + 1) % val) for rr in range(val)])
+                if p + 1 < val
+                else sample
+            )
+            chunks.append(arr(sample, (all_rows - p) % val * seen_now))
+            sample = t_next
+        e_next = jnp.roll(jnp.concatenate(chunks[::-1], 2), (all_rows + 1) * chunks[0].shape[2], 2)
+        return e_next
+
     seq_local, length, feat_local = tokens.shape
     stream = tokens.astype(jnp.float32)
     first_square = lax.psum(jnp.sum(stream * stream, axis=-1), "tp")
@@ -92,11 +109,12 @@
         preferred_element_type=jnp.float32,
     )
     hidden = (jax.nn.silu(gate_sum) * up_sum).astype(jnp.bfloat16)
-    partial_value = jnp.einsum(
-        "hor,rn->hon",
-        hidden,
-        lax.all_gather(down_weight, "fs", axis=1, tiled=True),
-        preferred_element_type=jnp.float32,
+    partial_value = _trace_node(
+        down_weight,
+        net_axis="fs",
+        arr=lambda own_block, offset: jnp.einsum(
+            "hor,rn->hon", hidden, own_block, preferred_element_type=jnp.float32
+        ),
     )
     summed = lax.psum_scatter(
         partial_value.astype(jnp.bfloat16), "tp", scatter_dimension=2, tiled=True

time: 486 us -> 440 us (0.905)
  waiting for transfers between devices: 418 us -> 333 us
  starting transfers between devices: 0.28 us -> 36 us
    all_gather x1 -> x0, waiting for transfers between devices: 107 us -> none  [local(): lax.all_gather(down_weight, 'fs', axis=1, tiled=True)]
    ppermute x0 -> x3, waiting for transfers between devices: none -> 100 us  [_trace_node(): lax.ppermute(sample, net_axis, [(rr, (rr + 1) % val) for rr in range(val)])]
    all_gather x1, waiting for transfers between devices: 108 us -> 45.2 us  [local(): lax.all_gather(gate_weight, 'fs', axis=0, tiled=True)]
    ppermute x0 -> x3, starting transfers between devices: none -> 35.8 us  [_trace_node(): lax.ppermute(sample, net_axis, [(rr, (rr + 1) % val) for rr in range(val)])]
    all_gather x1, waiting for transfers between devices: 17 us -> 0.01 us  [local(): features_full = lax.all_gather(normed_two, 'tp', axis=2, tiled=True)]
    dot_general x1 -> x5, matrix products: 11.3 us -> 13.2 us  [the longest x4 7.33 us: local(): jnp.einsum('hor,rn->hon', hidden, own_block, preferred_element_type=jnp.f...]
  transfers between devices with their start and end apart: 8 -> 10, of which waited for: 8 -> 8; matrix products, arithmetic and copies ran while one was open for 3% -> 5% of each run, Pallas kernels for 0% -> 0%
where the time goes in v1:
time: 440 us
  waiting for transfers between devices  333 us (76%)
  starting transfers between devices  36 us (8%)
  matrix products  24.8 us (6%)
  blocking collectives  23 us (5%)
  between operations  13.8 us (3%)
  other arithmetic  6.85 us (2%)
    all_gather x1, waiting for transfers between devices, local(): lax.all_gather(up_weight, 'fs', axis=0, tiled=True)  101 us
    ppermute x3, waiting for transfers between devices, _trace_node(): lax.ppermute(sample, net_axis, [(rr, (rr + 1) % val) for rr in range(val)])  100 us
    all_gather x1, waiting for transfers between devices, local(): lax.all_gather(gate_weight, 'fs', axis=0, tiled=True)  45.2 us
    ppermute x3, starting transfers between devices, _trace_node(): lax.ppermute(sample, net_axis, [(rr, (rr + 1) % val) for rr in range(val)])  35.8 us
    reduce_scatter x1, waiting for transfers between devices, local(): lax.psum_scatter(partial_value.astype(jnp.bfloat16), 'tp', scatter_dimens...  26.3 us
    all_gather x1, waiting for transfers between devices, local(): lax.all_gather(normed, 'tp', axis=2, tiled=True)  20.6 us
    all_gather x1, waiting for transfers between devices, local(): in_full = lax.all_gather(in_weight, 'fs', axis=0, tiled=True)  20 us
    all_gather x1, waiting for transfers between devices, local(): out_full = lax.all_gather(out_weight, 'fs', axis=0, tiled=True)  17 us
  transfers between devices with their start and end apart: 10, of which 8 were waited for; matrix products, arithmetic and copies ran while one was open for 5% of the time, Pallas kernels for 0%

profile of v1, /device:TPU:0, one launch (start us, length us, event | category | flops | bytes accessed | tf_op | source)
XLA Modules:
  0.0 439.6 jit_solution(15219113747891514002)
XLA Ops:
  6.5 0.0 copy-start
  6.5 0.0 all-gather.9.cloned.1.call-start
  6.5 0.7 all-gather.9.cloned.1.call-update
  7.3 0.0 all-gather.7.cloned.1.call-start
  7.3 1.2 fusion.16
  8.5 8.4 %psum.14 = f32[1,384]{1,0:T(1,128)S(1)} all-reduce(f32[1,384]{1,0:T(1,128)S(1)} %reduce_sum.23), channel_id=1, replica_groups=mesh['grp'=2,'fs'=4,'tp'=4] {'tp'}, use_global_device_ids=true, to_apply=%region_1.0 | all-reduce | flops 384 | bytes 3072 | tf_op jit(solution)/shard_map/psum | solution.py:43
  16.9 1.9 fusion.18
  18.8 0.0 all-gather.7.cloned.1.call-update
  18.8 0.0 all-gather.11.cloned.1.call-start
  18.8 0.7 all-gather.11.cloned.1.call-update
  19.5 0.0 all-gather.13.cloned.1.call-start
  19.6 20.0 %all-gather.9.cloned.1.call-done = bf16[2048,256]{1,0:T(8,128)(2,1)} async-done(((bf16[512,256]{1,0:T(8,128)(2,1)}), bf16[2048,256]{1,0:T(8,128)(2,1)}) %all-gather.9.cloned.1.call-update) | async-done | bytes 1048592 | tf_op jit(solution)/shard_map/all_gather | solution.py:47
  39.6 20.6 %all-gather.7.cloned.1.call-done = bf16[1,384,2048]{2,1,0:T(8,128)(2,1)} async-done(((bf16[1,384,512]{2,1,0:T(8,128)(2,1)}), bf16[1,384,2048]{2,1,0:T(8,128)(2,1)}) %all-gather.7.cloned.1.call-update) | async-done | bytes 1572880 | tf_op jit(solution)/shard_map/all_gather | solution.py:52
  60.2 2.3 fusion.13
  62.5 0.3 fusion.20
  62.8 0.1 copy.12
  63.0 0.1 fusion.59
  63.1 0.1 fusion.57
  63.1 0.1 fusion.58
  63.2 0.0 copy-start.3
  63.3 0.5 fusion.36
  63.8 0.0 copy-start.1
  63.8 0.1 reshape.233
  63.8 0.0 copy-done
  63.8 0.3 fusion.37
  64.1 0.0 copy-done.3
  64.1 0.1 fusion.35
  64.2 8.6 %all_gather.23 = bf16[1,384,1024]{1,2,0:T(8,128)(2,1)S(1)} all-gather(bf16[1,384,256]{1,2,0:T(8,128)(2,1)S(1)} %fusion.35), channel_id=1, replica_groups=mesh['grp'=2,'fs'=4,'tp'=4] {'tp'}, dimensions={2}, use_global_device_ids=true | all-gather | bytes 983040 | tf_op jit(solution)/shard_map/all_gather | solution.py:90
  72.8 0.0 copy-start.2
  72.8 17.0 %all-gather.11.cloned.1.call-done = bf16[1024,512]{1,0:T(8,128)(2,1)} async-done(((bf16[256,512]{1,0:T(8,128)(2,1)}), bf16[1024,512]{1,0:T(8,128)(2,1)}) %all-gather.11.cloned.1.call-update) | async-done | bytes 1048592 | tf_op jit(solution)/shard_map/all_gather | solution.py:86
  89.8 0.0 copy-done.1
  89.8 1.9 multiply_reduce_fusion
  91.8 6.1 %psum.15 = f32[1,384]{1,0:T(1,128)S(1)} all-reduce(f32[1,384]{1,0:T(1,128)S(1)} %reduce_sum.25), channel_id=1, replica_groups=mesh['grp'=2,'fs'=4,'tp'=4] {'tp'}, use_global_device_ids=true, to_apply=%region_5.6 | all-reduce | flops 384 | bytes 3072 | tf_op jit(solution)/shard_map/psum | solution.py:94
  97.9 0.0 copy-done.2
  97.9 0.9 multiply_convert_fusion
  98.8 0.0 copy-start.5
  98.8 0.0 all-gather.13.cloned.1.call-update
  98.8 0.0 all-gather.15.cloned.1.call-start
  98.8 0.5 all-gather.15.cloned.1.call-update
  99.4 0.0 all-gather.17.cloned.1.call-start
  99.4 0.5 all-gather.17.cloned.1.call-update
  100.0 0.0 reduce-scatter.2.cloned.1.call-start
  100.0 0.1 copy-done.5
  100.1 1.1 collective-permute-start
  101.3 37.7 %collective-permute-done = bf16[1408,512]{1,0:T(8,128)(2,1)} collective-permute-done((bf16[1408,512]{1,0:T(8,128)(2,1)S(1)}, bf16[1408,512]{1,0:T(8,128)(2,1)}, u32[]{:S(2)}, u32[]{:S(2)}) %collective-permute-start) | collective-permute-done | bytes 1441824 | tf_op jit(solution)/shard_map/ppermute | solution.py:32
  138.9 2.9 collective-permute-start.1
  141.8 62.8 %collective-permute-done.1 = bf16[1408,512]{1,0:T(8,128)(2,1)} collective-permute-done((bf16[1408,512]{1,0:T(8,128)(2,1)}, bf16[1408,512]{1,0:T(8,128)(2,1)}, u32[]{:S(2)}, u32[]{:S(2)}) %collective-permute-start.1) | collective-permute-done | bytes 1441824 | tf_op jit(solution)/shard_map/ppermute | solution.py:32
  204.6 31.7 %collective-permute-start.2 = (bf16[1408,512]{1,0:T(8,128)(2,1)}, bf16[1408,512]{1,0:T(8,128)(2,1)}, u32[]{:S(2)}, u32[]{:S(2)}) collective-permute-start(bf16[1408,512]{1,0:T(8,128)(2,1)} %collective-permute-done.1), channel_id=1, source_target_pairs={{0,4},{4,8},{8,12},{12,0},{1,5},{5,9},{9,13},{13,1},{2,6},{6,10},{... | collective-permute-start | bytes 4325384 | tf_op jit(solution)/shard_map/ppermute | solution.py:32
  236.3 45.2 %all-gather.15.cloned.1.call-done = bf16[2048,1408]{1,0:T(8,128)(2,1)} async-done(((bf16[512,1408]{1,0:T(8,128)(2,1)}), bf16[2048,1408]{1,0:T(8,128)(2,1)}) %all-gather.15.cloned.1.call-update) | async-done | bytes 5767184 | tf_op jit(solution)/shard_map/all_gather | solution.py:102
  281.5 7.2 %fusion.2 = f32[384,1408]{1,0:T(8,128)} fusion(bf16[2048,1408]{1,0:T(8,128)(2,1)} %all-gather.15.cloned.1.call-done, bf16[1,384,2048]{2,1,0:T(8,128)(2,1)} %all-gather.13.cloned.1.call-done), kind=kOutput, calls=%fused_computation.4 | convolution fusion | flops 2214592512 | bytes 9502720 | tf_op jit(solution)/shard_map/slk,kf->slf/dot_general | solution.py:99
  288.7 101.0 %all-gather.17.cloned.1.call-done = bf16[2048,1408]{1,0:T(8,128)(2,1)} async-done(((bf16[512,1408]{1,0:T(8,128)(2,1)}), bf16[2048,1408]{1,0:T(8,128)(2,1)}) %all-gather.17.cloned.1.call-update) | async-done | bytes 5767184 | tf_op jit(solution)/shard_map/all_gather | solution.py:108
  389.7 0.0 copy-done.4
  389.7 5.8 %fusion = bf16[384,1408]{1,0:T(8,128)(2,1)S(1)} fusion(bf16[2048,1408]{1,0:T(8,128)(2,1)} %all-gather.17.cloned.1.call-done, f32[384,1408]{1,0:T(8,128)} %fusion.2, bf16[1,384,2048]{2,1,0:T(8,128)(2,1)S(1)} %copy-done.4), kind=kOutput, calls=%fused_computation.2 | convolution fusion | flops 2217836544 | bytes 10584064 | tf_op jit(solution)/shard_map/slk,kf->slf/dot_general | solution.py:105
  395.5 0.0 collective-permute-done.2
  395.6 2.1 constant_dynamic-update-slice_fusion.7
  397.7 2.1 constant_dynamic-update-slice_fusion.6
  399.9 0.0 copy-start.6
  399.9 2.3 constant_dynamic-update-slice_fusion.5
  402.1 0.0 copy-done.6
  402.1 0.8 constant_dynamic-update-slice_fusion.4
  403.1 1.4 dynamic-slice_convert_fusion
  404.5 0.0 reduce-scatter.2.cloned.1.call-update
  404.5 26.3 %reduce-scatter.2.cloned.1.call-done = bf16[1,384,512]{2,1,0:T(8,128)(2,1)} async-done(((bf16[1,384,2048]{2,1,0:T(8,128)(2,1)}), bf16[1,384,512]{2,1,0:T(8,128)(2,1)}) %reduce-scatter.2.cloned.1.call-update) | async-done | bytes 393232 | tf_op jit(solution)/shard_map/reduce_scatter | solution.py:119
  430.8 1.9 add_convert_fusion
  (23 shorter events, 0.4 us)
Async XLA Ops:
  6.5 57.3 %copy-start = (bf16[2,128,128]{2,1,0:T(8,128)(2,1)S(1)}, bf16[2,128,128]{2,1,0:T(8,128)(2,1)}, u32[]{:S(2)}) copy-start(bf16[2,128,128]{2,1,0:T(8,128)(2,1)} %param.13) | copy-start | bytes 196612
  6.5 33.1 %all-gather.9.cloned.1.call-start = ((), (), s32[]{:S(2)}) async-start(), calls=%async_computation.2 | async-start | bytes 1310720 | tf_op jit(solution)/shard_map/all_gather | solution.py:47
  7.3 53.0 %all-gather.7.cloned.1.call-start = ((), (), s32[]{:S(2)}) async-start(), calls=%async_computation.1 | async-start | bytes 1966080 | tf_op jit(solution)/shard_map/all_gather | solution.py:52
  18.8 71.0 %all-gather.11.cloned.1.call-start = ((), (), s32[]{:S(2)}) async-start(), calls=%async_computation.3 | async-start | bytes 1310720 | tf_op jit(solution)/shard_map/all_gather | solution.py:86
  19.5 216.8 %all-gather.13.cloned.1.call-start = ((), (), s32[]{:S(2)}) async-start(), calls=%async_computation.4 | async-start | bytes 1966080 | tf_op jit(solution)/shard_map/all_gather | solution.py:98
  63.2 0.9 copy-start.3
  63.8 26.1 %copy-start.1 = (bf16[1,384,512]{2,1,0:T(8,128)(2,1)S(1)}, bf16[1,384,512]{2,1,0:T(8,128)(2,1)}, u32[]{:S(2)}) copy-start(bf16[1,384,512]{2,1,0:T(8,128)(2,1)} %param.10) | copy-start | bytes 1179652
  72.8 25.1 %copy-start.2 = (f32[512]{0:T(512)S(1)}, f32[512]{0:T(512)}, u32[]{:S(2)}) copy-start(f32[512]{0:T(512)} %param.16) | copy-start | bytes 6148
  98.8 1.4 copy-start.5
  98.8 182.7 %all-gather.15.cloned.1.call-start = ((), (), s32[]{:S(2)}) async-start(), calls=%async_computation.5 | async-start | bytes 7208960 | tf_op jit(solution)/shard_map/all_gather | solution.py:102
  99.4 290.3 %all-gather.17.cloned.1.call-start = ((), (), s32[]{:S(2)}) async-start(), calls=%async_computation.6 | async-start | bytes 7208960 | tf_op jit(solution)/shard_map/all_gather | solution.py:108
  100.0 330.9 %reduce-scatter.2.cloned.1.call-start = ((), (), s32[]{:S(2)}) async-start(), calls=%async_computation.7 | async-start | bytes 1966080 | tf_op jit(solution)/shard_map/reduce_scatter | solution.py:119
  100.1 38.8 %collective-permute-start = (bf16[1408,512]{1,0:T(8,128)(2,1)S(1)}, bf16[1408,512]{1,0:T(8,128)(2,1)}, u32[]{:S(2)}, u32[]{:S(2)}) collective-permute-start(bf16[1408,512]{1,0:T(8,128)(2,1)S(1)} %copy-done.5), channel_id=1, source_target_pairs={{0,4},{4,8},{8,12},{12,0},{1,5},{5,9},{9,13},{13,1},{2,6},{6,10},{... | collective-permute-start | bytes 4325384 | tf_op jit(solution)/shard_map/ppermute | solution.py:32
  138.9 65.7 %collective-permute-start.1 = (bf16[1408,512]{1,0:T(8,128)(2,1)}, bf16[1408,512]{1,0:T(8,128)(2,1)}, u32[]{:S(2)}, u32[]{:S(2)}) collective-permute-start(bf16[1408,512]{1,0:T(8,128)(2,1)} %collective-permute-done), channel_id=1, source_target_pairs={{0,4},{4,8},{8,12},{12,0},{1,5},{5,9},{9,13},{13,1},{2,6},{6,10},{... | collective-permute-start | bytes 4325384 | tf_op jit(solution)/shard_map/ppermute | solution.py:32
  204.6 190.9 %collective-permute-start.2 = (bf16[1408,512]{1,0:T(8,128)(2,1)}, bf16[1408,512]{1,0:T(8,128)(2,1)}, u32[]{:S(2)}, u32[]{:S(2)}) collective-permute-start(bf16[1408,512]{1,0:T(8,128)(2,1)} %collective-permute-done.1), channel_id=1, source_target_pairs={{0,4},{4,8},{8,12},{12,0},{1,5},{5,9},{9,13},{13,1},{2,6},{6,10},{... | collective-permute-start | bytes 4325384 | tf_op jit(solution)/shard_map/ppermute | solution.py:32
  236.3 153.4 %copy-start.4 = (bf16[1,384,2048]{2,1,0:T(8,128)(2,1)S(1)}, bf16[1,384,2048]{2,1,0:T(8,128)(2,1)}, u32[]{:S(2)}) copy-start(bf16[1,384,2048]{2,1,0:T(8,128)(2,1)} %all-gather.13.cloned.1.call-done) | copy-start | bytes 4718596
  399.9 2.3 copy-start.6
Sparse Core Ops, SparseCore 0:
  8.9 30.6 all-gather.8
  41.2 18.9 all-gather.6
  61.8 27.9 all-gather.10
  98.9 18.8 all-gather.12
  119.2 162.2 all-gather.14
  282.9 106.7 all-gather.16
  404.6 26.1 reduce-scatter.1
